TPU v7x, 32 devices: a whole 2x2x4 slice. The times are simulated.
32 devices in a mesh: sp: 4 (over z), fs: 4 (over y, x), tp: 2 (over core).
Axes of the slice: x: 2, y: 2, z: 4, core: 2. Of those that a mesh axis runs over, the one named last changes fastest.
Arguments:
- tokens: bfloat16 [4, 1024, 2048], P('fs', 'sp'), may hold values from -6 to 6
- norm_gain: float32 [2048], replicated, may hold values from 0.1 to 1.9
- query_weight: bfloat16 [2048, 1024], P(('sp', 'fs'), 'tp'), may hold values from -0.125 to 0.125
- key_weight: bfloat16 [2048, 1024], P(('sp', 'fs'), 'tp'), may hold values from -0.125 to 0.125
- value_weight: bfloat16 [2048, 1024], P(('sp', 'fs'), 'tp'), may hold values from -0.125 to 0.125
- outgate_weight: bfloat16 [2048, 1024], P(('sp', 'fs'), 'tp'), may hold values from -0.125 to 0.125
- gate_weight: bfloat16 [4, 8, 2048], P(None, 'tp'), may hold values from -0.125 to 0.125
- gate_bias: float32 [4, 8], P(None, 'tp'), may hold values from -1 to 100
- decay_extra: float32 [4, 2, 8, 1024], P('fs', None, 'tp', 'sp'), may hold values from -0.75 to 0
- init_memory: float32 [4, 2, 8, 128, 128], P('fs', None, 'tp'), may hold values from -48 to 48
- init_normalizer: float32 [4, 2, 8, 128], P('fs', None, 'tp'), may hold values from -48 to 48
- head_gain: float32 [8, 128], P('tp'), may hold values from 0.1 to 1.9
- pool_weight: bfloat16 [2048, 2048], P(('sp', 'fs'), 'tp'), may hold values from -0.125 to 0.125
- mem_out_weight: bfloat16 [2048, 1024], P(('sp', 'fs'), 'tp'), may hold values from -0.1875 to 0.1875
- pool_out_weight: bfloat16 [2048, 2048], P(('sp', 'fs'), 'tp'), may hold values from -0.125 to 0.125
Outputs:
- mixed: bfloat16 [4, 1024, 2048], P('fs', ('sp', 'tp'))
All inputs are finite; a program needn't handle non-finite values.
Results may differ from a plain program's by a relative error of at most 0.014.
Values may be sent and summed in bfloat16 or wider, within the bound.
A program may use at most 64 MiB of HBM per device.

v0:
```python
import math
import jax
import jax.numpy as jnp
from jax import lax
from jax.sharding import PartitionSpec as P

HALO = 8
norm_eps = 1e-06
exact_mode = lax.Precision.HIGHEST


def carried_in(x, axis, combine, identity, reverse):
    length, position = (lax.axis_size(axis), lax.axis_index(axis))
    everything = jax.tree.map(lambda part: lax.all_gather(part, axis), x)
    start = jax.tree.map(
        lambda part, zero: jnp.broadcast_to(jnp.asarray(zero, part.dtype), part.shape), x, identity
    )

    def lap(k, before):
        at = length - 1 - k if reverse else k
        reached = at > position if reverse else at < position
        new = combine(before, jax.tree.map(lambda part: part[at], everything))
        return jax.tree.map(lambda a, b: jnp.where(reached, a, b), new, before)

    return lax.fori_loop(0, length, lap, start)


def padded_2(block, sides, width):
    for axis, dim in sides:
        count = lax.axis_size(axis)
        forward = [(i, i + 1) for i in range(count - 1)]
        backward = [(target, source) for source, target in forward]
        low = lax.ppermute(
            lax.slice_in_dim(block, block.shape[dim] - width, None, axis=dim), axis, forward
        )
        high = lax.ppermute(lax.slice_in_dim(block, 0, width, axis=dim), axis, backward)
        block = jnp.concatenate([low, block, high], axis=dim)
    return block


def block_output(
    query_rows, key_rows, value_rows, input_gate, log_forget, memory, normalizer, stabilizer
):
    block_len = query_rows.shape[1]
    key_scale = key_rows.shape[-1] ** (-0.5)
    lower_mask = jnp.tril(jnp.ones((block_len, block_len), dtype=bool))
    summed = jnp.cumsum(log_forget, axis=-1)
    log_decay = jnp.where(
        lower_mask, summed[:, :, None] - summed[:, None, :] + input_gate[:, None, :], -jnp.inf
    )
    log_carry = stabilizer[:, None] + summed
    running_max = jnp.maximum(log_carry, jnp.max(log_decay, axis=-1))
    scores = (
        jnp.einsum("btd,bsd->bts", query_rows, key_rows, preferred_element_type=jnp.float32)
        * key_scale
    )
    inner_weight = jnp.exp(log_decay - running_max[:, :, None]) * scores
    weight_rounded = inner_weight.astype(jnp.bfloat16)
    carry_weight = jnp.exp(log_carry - running_max)
    query_wide = query_rows.astype(jnp.float32)
    numerator = carry_weight[:, :, None] * jnp.einsum(
        "bed,btd->bte", memory, query_wide, precision=exact_mode
    )
    numerator = numerator + jnp.einsum(
        "bts,bse->bte", weight_rounded, value_rows, preferred_element_type=jnp.float32
    )
    denominator = carry_weight * jnp.einsum(
        "bd,btd->bt", normalizer, query_wide, precision=exact_mode
    )
    denominator = denominator + jnp.sum(inner_weight, axis=-1)
    return numerator / jnp.maximum(jnp.abs(denominator), jnp.exp(-running_max))[:, :, None]


def block_summary(key_rows, value_rows, input_gate, log_forget):
    key_wide = key_rows.astype(jnp.float32) * key_rows.shape[-1] ** (-0.5)
    summed = jnp.cumsum(log_forget, axis=-1)
    forget_total = summed[:, -1]
    log_weight = forget_total[:, None] - summed + input_gate
    running_max = jnp.max(log_weight, axis=-1)
    weights = jnp.exp(log_weight - running_max[:, None])
    memory = jnp.einsum(
        "bse,bsd->bed",
        weights[:, :, None] * value_rows.astype(jnp.float32),
        key_wide,
        precision=exact_mode,
    )
    normalizer = jnp.einsum("bs,bsd->bd", weights, key_wide, precision=exact_mode)
    return (memory, normalizer, running_max, forget_total)


def combine(earlier, latter):
    early_memory, early_norm, early_max, early_total = earlier
    late_memory, late_norm, late_max, late_total = latter
    joint_max = jnp.maximum(early_max + late_total, late_max)
    early_scale = jnp.exp(early_max + late_total - joint_max)
    late_scale = jnp.exp(late_max - joint_max)
    memory = early_scale[:, None, None] * early_memory + late_scale[:, None, None] * late_memory
    normalizer = early_scale[:, None] * early_norm + late_scale[:, None] * late_norm
    return (memory, normalizer, joint_max, early_total + late_total)


def span_sweep(
    query_rows, key_rows, value_rows, input_gate, log_forget, memory, normalizer, stabilizer, span
):
    block_count = query_rows.shape[1] // span

    def to_blocks(array):
        shaped = array.reshape((array.shape[0], block_count, span) + array.shape[2:])
        return jnp.moveaxis(shaped, 1, 0)

    def advance(carried, pieces):
        query_blk, key_blk, value_blk, gate_blk, forget_blk = pieces
        result = block_output(
            query_blk, key_blk, value_blk, gate_blk, forget_blk, carried[0], carried[1], carried[2]
        )
        return (combine(carried, block_summary(key_blk, value_blk, gate_blk, forget_blk)), result)

    initial = (memory, normalizer, stabilizer, jnp.zeros_like(stabilizer))
    ignored, outputs = lax.scan(
        advance,
        initial,
        tuple(
            (
                to_blocks(array)
                for array in (query_rows, key_rows, value_rows, input_gate, log_forget)
            )
        ),
    )
    return jnp.moveaxis(outputs, 0, 1).reshape(query_rows.shape[:2] + (value_rows.shape[2],))


def reverse_time(array):
    return jnp.flip(array, axis=1)


def to_heads(matrix, head_count):
    shaped = matrix.reshape(matrix.shape[0], head_count, matrix.shape[1] // head_count)
    return shaped.transpose(1, 0, 2)


def pool_window(padded, positions, channels, seq_len, group_size):
    row_count = positions.shape[0]
    group_index = channels // group_size
    reach_left = jnp.left_shift(jnp.ones_like(group_index), group_index)
    reach_right = reach_left - 1
    window_sum = jnp.zeros((row_count, channels.shape[0]), jnp.float32)
    for offset in range(-HALO, HALO):
        inside = ((offset >= -reach_left) & (offset <= reach_right)).astype(jnp.float32)
        window_sum = window_sum + inside * padded[HALO + offset : HALO + offset + row_count]
    first_pos = jnp.maximum(positions[:, None] - reach_left[None, :], 0)
    last_pos = jnp.minimum(positions[:, None] + reach_right[None, :], seq_len - 1)
    counted = (last_pos - first_pos + 1).astype(jnp.float32)
    centre = padded[HALO : HALO + row_count]
    return (window_sum / counted - centre).astype(jnp.bfloat16)


def per_device(
    tokens,
    norm_gain,
    query_weight,
    key_weight,
    value_weight,
    outgate_weight,
    gate_weight,
    gate_bias,
    decay_extra,
    init_memory,
    init_normalizer,
    head_gain,
    pool_weight,
    mem_out_weight,
    pool_out_weight,
):
    block_len = tokens.shape[1]
    model_width = tokens.shape[2]
    head_count, head_width = head_gain.shape
    span = math.gcd(block_len, 256)
    flattened = tokens[0].astype(jnp.float32)
    normed = (
        flattened
        * lax.rsqrt(jnp.mean(flattened * flattened, axis=-1, keepdims=True) + norm_eps)
        * norm_gain
    ).astype(jnp.bfloat16)
    zero_start = tuple(
        (
            jnp.zeros((block_len, weight.shape[1]), jnp.float32)
            for weight in (query_weight, key_weight, value_weight, outgate_weight, pool_weight)
        )
    )
    zero_start = zero_start + (
        jnp.zeros((model_width, mem_out_weight.shape[1]), jnp.bfloat16),
        jnp.zeros((model_width, pool_out_weight.shape[1]), jnp.bfloat16),
    )
    line_query, line_key, line_value, line_outgate, line_pool, line_mem_out, line_pool_out = (
        lax.all_gather(query_weight, "fs", axis=0, tiled=True),
        lax.all_gather(key_weight, "fs", axis=0, tiled=True),
        lax.all_gather(value_weight, "fs", axis=0, tiled=True),
        lax.all_gather(outgate_weight, "fs", axis=0, tiled=True),
        lax.all_gather(pool_weight, "fs", axis=0, tiled=True),
        lax.all_gather(mem_out_weight, "fs", axis=0, tiled=True),
        lax.all_gather(pool_out_weight, "fs", axis=0, tiled=True),
    )
    pieces = (
        lax.all_gather(line_query, "sp", axis=0, tiled=True),
        lax.all_gather(line_key, "sp", axis=0, tiled=True),
        lax.all_gather(line_value, "sp", axis=0, tiled=True),
        lax.all_gather(line_outgate, "sp", axis=0, tiled=True),
        lax.all_gather(line_pool, "sp", axis=0, tiled=True),
        lax.all_gather(line_mem_out, "sp", axis=0, tiled=True),
        lax.all_gather(line_pool_out, "sp", axis=0, tiled=True),
    )
    partial_sums = tuple(
        (
            jnp.dot(normed, weight_rows, preferred_element_type=jnp.float32)
            for weight_rows in pieces[:5]
        )
    )
    collected = tuple((weight_rows for weight_rows in pieces[5:]))
    folded = partial_sums + collected
    query_proj, key_proj, value_proj, outgate, pool_input = tuple(
        (running.astype(jnp.bfloat16) for running in folded[:5])
    )
    mem_weight_all = folded[5]
    pool_weight_all = folded[6]
    gate_pre = lax.dot_general(
        normed,
        gate_weight.reshape(4 * head_count, model_width),
        (((1,), (1,)), ((), ())),
        preferred_element_type=jnp.float32,
    ) + gate_bias.reshape(4 * head_count)
    gate_pre = gate_pre.reshape(block_len, 4, head_count).transpose(1, 2, 0)
    query_heads = to_heads(query_proj, head_count)
    key_heads = to_heads(key_proj, head_count)
    value_heads = to_heads(value_proj, head_count)
    forward_forget = jax.nn.log_sigmoid(gate_pre[1]) + decay_extra[0, 0]
    backward_forget = jax.nn.log_sigmoid(gate_pre[3]) + decay_extra[0, 1]
    zero_rows = jnp.zeros((head_count,), jnp.float32)
    identity = (
        jnp.zeros((head_count, head_width, head_width), jnp.float32),
        jnp.zeros((head_count, head_width), jnp.float32),
        jnp.full((head_count,), -1e30, jnp.float32),
        zero_rows,
    )
    front_memory, front_norm, front_max, front_total = block_summary(
        key_heads, value_heads, gate_pre[0], forward_forget
    )
    prefix = carried_in(
        (front_memory, front_norm, front_max, front_total), "sp", combine, identity, False
    )
    incoming = combine((init_memory[0, 0], init_normalizer[0, 0], zero_rows, zero_rows), prefix)
    forward_out = span_sweep(
        query_heads,
        key_heads,
        value_heads,
        gate_pre[0],
        forward_forget,
        incoming[0],
        incoming[1],
        incoming[2],
        span,
    )
    back_query = reverse_time(query_heads)
    back_key = reverse_time(key_heads)
    back_value = reverse_time(value_heads)
    back_gate = reverse_time(gate_pre[2])
    back_forget = reverse_time(backward_forget)
    rear_memory, rear_norm, rear_max, rear_total = block_summary(
        back_key, back_value, back_gate, back_forget
    )
    suffix = carried_in(
        (rear_memory, rear_norm, rear_max, rear_total), "sp", combine, identity, True
    )
    back_incoming = combine(
        (init_memory[0, 1], init_normalizer[0, 1], zero_rows, zero_rows), suffix
    )
    backward_out = reverse_time(
        span_sweep(
            back_query,
            back_key,
            back_value,
            back_gate,
            back_forget,
            back_incoming[0],
            back_incoming[1],
            back_incoming[2],
            span,
        )
    )
    summed_dirs = (forward_out + backward_out).transpose(1, 0, 2)
    normed_heads = (
        summed_dirs
        * lax.rsqrt(jnp.mean(summed_dirs * summed_dirs, axis=-1, keepdims=True) + norm_eps)
        * head_gain
    )
    out_gate = jax.nn.sigmoid(
        outgate.astype(jnp.float32).reshape(block_len, head_count, head_width)
    )
    memory_out = (
        (normed_heads * out_gate).astype(jnp.bfloat16).reshape(block_len, head_count * head_width)
    )
    padded = padded_2(pool_input, (("sp", 0),), HALO).astype(jnp.float32)
    feature_count = pool_input.shape[1]
    positions = lax.axis_index("sp") * block_len + jnp.arange(block_len, dtype=jnp.int32)
    channels = lax.axis_index("tp") * feature_count + jnp.arange(feature_count, dtype=jnp.int32)
    pool_out = pool_window(
        padded, positions, channels, block_len * lax.axis_size("sp"), model_width // 4
    )
    own_rows = block_len // lax.axis_size("tp")
    result = lax.dot_general(
        memory_out, mem_weight_all, (((1,), (1,)), ((), ())), preferred_element_type=jnp.float32
    )
    mixed = lax.psum_scatter(
        (
            result
            + lax.dot_general(
                pool_out,
                pool_weight_all,
                (((1,), (1,)), ((), ())),
                preferred_element_type=jnp.float32,
            )
        ).astype(jnp.bfloat16),
        "tp",
        scatter_dimension=0,
        tiled=True,
    )
    return mixed.reshape(1, own_rows, model_width)


def solution(mesh):
    placed = (
        P("fs", "sp", None),
        P(),
        P(("sp", "fs"), "tp"),
        P(("sp", "fs"), "tp"),
        P(("sp", "fs"), "tp"),
        P(("sp", "fs"), "tp"),
        P(None, "tp", None),
        P(None, "tp"),
        P("fs", None, "tp", "sp"),
        P("fs", None, "tp", None, None),
        P("fs", None, "tp", None),
        P("tp", None),
        P(("sp", "fs"), "tp"),
        P(("sp", "fs"), "tp"),
        P(("sp", "fs"), "tp"),
    )
    return jax.shard_map(
        per_device,
        mesh=mesh,
        in_specs=placed,
        out_specs=P("fs", ("sp", "tp"), None),
        check_vma=False,
    )
```

profile of v0, /device:TPU:0, one launch (start us, length us, event | category | flops | bytes accessed | tf_op | source)
XLA Modules:
  0.0 544.0 jit_solution(11762868126986876266)
XLA Ops:
  6.5 13.3 %all_gather.89 = bf16[512,512]{1,0:T(8,128)(2,1)} all-gather(bf16[128,512]{1,0:T(8,128)(2,1)} %param.22), channel_id=1, replica_groups=mesh['sp'=4,'fs'=4,'tp'=2] {'fs'}, dimensions={0}, use_global_device_ids=true | all-gather | bytes 655360 | tf_op jit(solution)/shard_map/all_gather | solution.py:196
  19.9 11.6 %all_gather.87 = bf16[512,512]{1,0:T(8,128)(2,1)} all-gather(bf16[128,512]{1,0:T(8,128)(2,1)} %param.23), channel_id=1, replica_groups=mesh['sp'=4,'fs'=4,'tp'=2] {'fs'}, dimensions={0}, use_global_device_ids=true | all-gather | bytes 655360 | tf_op jit(solution)/shard_map/all_gather | solution.py:197
  31.6 0.7 all-gather.32.cloned.1.call-update
  32.9 10.5 %all_gather.95 = bf16[512,512]{1,0:T(8,128)(2,1)} all-gather(bf16[128,512]{1,0:T(8,128)(2,1)S(1)} %copy-done.3), channel_id=1, replica_groups=mesh['sp'=4,'fs'=4,'tp'=2] {'fs'}, dimensions={0}, use_global_device_ids=true | all-gather | bytes 655360 | tf_op jit(solution)/shard_map/all_gather | solution.py:195
  43.5 10.5 %all_gather.104 = bf16[512,512]{1,0:T(8,128)(2,1)} all-gather(bf16[128,512]{1,0:T(8,128)(2,1)S(1)} %copy-done.4), channel_id=1, replica_groups=mesh['sp'=4,'fs'=4,'tp'=2] {'fs'}, dimensions={0}, use_global_device_ids=true | all-gather | bytes 655360 | tf_op jit(solution)/shard_map/all_gather | solution.py:198
  55.1 1.2 reduce-window.24
  57.2 8.7 %all-gather.24.cloned.1.call-done = bf16[2048,512]{1,0:T(8,128)(2,1)} async-done(((bf16[512,512]{1,0:T(8,128)(2,1)}), bf16[2048,512]{1,0:T(8,128)(2,1)}) %all-gather.24.cloned.1.call-update) | async-done | bytes 2097168 | tf_op jit(solution)/shard_map/all_gather | solution.py:205
  65.9 2.3 fusion.36
  68.3 43.7 %all-gather.22.cloned.1.call-done = bf16[2048,512]{1,0:T(8,128)(2,1)} async-done(((bf16[512,512]{1,0:T(8,128)(2,1)}), bf16[2048,512]{1,0:T(8,128)(2,1)}) %all-gather.22.cloned.1.call-update) | async-done | bytes 2097168 | tf_op jit(solution)/shard_map/all_gather | solution.py:206
  112.0 2.3 fusion.35
  114.3 1.9 fusion.71
  116.5 1.2 reduce-window.26
  119.5 1.9 fusion.65
  121.5 17.7 %all-gather.32.cloned.1.call-done = bf16[512,1024]{1,0:T(8,128)(2,1)} async-done(((bf16[128,1024]{1,0:T(8,128)(2,1)}), bf16[512,1024]{1,0:T(8,128)(2,1)}) %all-gather.32.cloned.1.call-update) | async-done | bytes 1048592 | tf_op jit(solution)/shard_map/all_gather | solution.py:199
  139.3 28.2 %all-gather.36.cloned.1.call-done = bf16[512,1024]{1,0:T(8,128)(2,1)} async-done(((bf16[128,1024]{1,0:T(8,128)(2,1)}), bf16[512,1024]{1,0:T(8,128)(2,1)}) %all-gather.36.cloned.1.call-update) | async-done | bytes 1048592 | tf_op jit(solution)/shard_map/all_gather | solution.py:201
  167.5 10.6 %all_gather.106 = bf16[512,512]{1,0:T(8,128)(2,1)} all-gather(bf16[128,512]{1,0:T(8,128)(2,1)S(1)} %copy-done.5), channel_id=1, replica_groups=mesh['sp'=4,'fs'=4,'tp'=2] {'fs'}, dimensions={0}, use_global_device_ids=true | all-gather | bytes 655360 | tf_op jit(solution)/shard_map/all_gather | solution.py:200
  180.2 0.6 and_convert_fusion.4
  180.8 0.6 and_convert_fusion.6
  181.4 0.6 and_convert_fusion.8
  182.6 0.6 and_convert_fusion.12
  185.9 12.3 %all-reduce.4 = (f32[16]{0:T(128)S(1)}, f32[16]{0:T(128)S(1)}, f32[16]{0:T(128)S(1)}, f32[16]{0:T(128)S(1)}) all-reduce(f32[16]{0:T(128)S(1)} %dynamic-update-slice.2, f32[16]{0:T(128)S(1)} %dynamic-update-slice.3, f32[16]{0:T(128)S(1)} %dynamic-update-slice, f32[16]{0:T(128)S(1)} %dynamic-update-slice.1), channel_id=6, replica_groups=mesh['sp'=4,'fs'=4,'tp'=2] {'sp'}, use_global_device_ids=true, to_apply=%add.2 | all-reduce | flops 64 | bytes 512
  198.2 0.7 reshape.473
  199.0 0.7 reshape.477
  200.2 0.7 fusion.58
  201.4 12.5 %all-gather.8 = f32[4,4,128]{2,1,0:T(4,128)S(1)} all-gather(f32[1,4,128]{2,1,0:T(4,128)S(1)} %bitcast.306), channel_id=5, replica_groups=mesh['sp'=4,'fs'=4,'tp'=2] {'sp'}, dimensions={0}, use_global_device_ids=true | all-gather | bytes 10240 | tf_op jit(solution)/shard_map/all_gather | solution.py:14
  214.2 12.1 %all-gather.9 = f32[4,4,128]{2,1,0:T(4,128)S(1)} all-gather(f32[1,4,128]{2,1,0:T(4,128)S(1)} %bitcast.302), channel_id=9, replica_groups=mesh['sp'=4,'fs'=4,'tp'=2] {'sp'}, dimensions={0}, use_global_device_ids=true | all-gather | bytes 10240 | tf_op jit(solution)/shard_map/all_gather | solution.py:14
  226.4 2.3 fusion.37
  229.1 31.8 %all-gather.28.cloned.1.call-done = bf16[2048,512]{1,0:T(8,128)(2,1)} async-done(((bf16[512,512]{1,0:T(8,128)(2,1)}), bf16[2048,512]{1,0:T(8,128)(2,1)}) %all-gather.28.cloned.1.call-update) | async-done | bytes 2097168 | tf_op jit(solution)/shard_map/all_gather | solution.py:207
  260.9 3.2 fusion.34
  264.1 1.2 copy.60
  265.4 23.9 %all-gather.40.cloned.1.call-done = f32[16,128,128]{2,1,0:T(8,128)} async-done(((f32[4,128,128]{2,1,0:T(8,128)}), f32[16,128,128]{2,1,0:T(8,128)}) %all-gather.40.cloned.1.call-update) | async-done | bytes 1048592 | tf_op jit(solution)/shard_map/all_gather | solution.py:14
  289.3 7.4 %while.12 = (s32[]{:T(128)}, f32[4,128,128]{2,1,0:T(8,128)S(1)}, f32[4,128]{1,0:T(4,128)S(1)}, f32[4]{0:T(128)S(1)}, f32[4]{0:T(128)S(1)}, /*index=5*/s32[]{:T(1...) while((s32[]{:T(128)}, f32[4,128,128]{2,1,0:T(8,128)S(1)}, ...), condition=%wide.region_5.6_spmd.clone, body=%wide.region_4.5_spmd.clone.sunk | while | flops 330284 | bytes 792973 | solution.py:25
  289.3 0.7 broadcast_select_fusion.10
  290.0 1.1 fusion.157
  291.1 0.7 broadcast_select_fusion.10
  291.8 1.1 fusion.157
  293.0 0.7 broadcast_select_fusion.10
  293.7 1.1 fusion.157
  294.9 0.7 broadcast_select_fusion.10
  295.5 1.1 fusion.157
  297.8 2.3 fusion.133
  300.1 18.2 %all-gather.42.cloned.1.call-done = f32[16,128,128]{2,1,0:T(8,128)} async-done(((f32[4,128,128]{2,1,0:T(8,128)}), f32[16,128,128]{2,1,0:T(8,128)}) %all-gather.42.cloned.1.call-update) | async-done | bytes 1048592 | tf_op jit(solution)/shard_map/all_gather | solution.py:14
  318.3 7.5 %while.13 = (s32[]{:T(128)}, f32[4,128,128]{2,1,0:T(8,128)S(1)}, f32[4,128]{1,0:T(4,128)S(1)}, f32[4]{0:T(128)S(1)}, f32[4]{0:T(128)S(1)}, /*index=5*/s32[]{:T(1...) while((s32[]{:T(128)}, f32[4,128,128]{2,1,0:T(8,128)S(1)}, ...), condition=%wide.region_12.13_spmd.clone, body=%wide.region_11.12_spmd.clone.sunk | while | flops 330288 | bytes 793035 | solution.py:25
  318.3 0.7 broadcast_select_fusion.11
  319.0 1.1 fusion.159
  320.2 0.7 broadcast_select_fusion.11
  320.9 1.1 fusion.159
  322.0 0.7 broadcast_select_fusion.11
  322.7 1.1 fusion.159
  323.9 0.7 broadcast_select_fusion.11
  324.6 1.1 fusion.159
  327.7 1.2 fusion.25
  329.0 5.0 rev.26
  334.4 1.7 multiply_reduce_fusion
  336.1 63.9 %all-gather.34.cloned.1.call-done = bf16[2048,1024]{1,0:T(8,128)(2,1)} async-done(((bf16[512,1024]{1,0:T(8,128)(2,1)}), bf16[2048,1024]{1,0:T(8,128)(2,1)}) %all-gather.34.cloned.1.call-update) | async-done | bytes 4194320 | tf_op jit(solution)/shard_map/all_gather | solution.py:208
  400.0 3.5 convolution_convert_fusion
  403.7 1.3 collective-permute-start
  405.0 1.3 collective-permute-start.1
  406.4 4.2 collective-permute-done.1
  410.8 69.9 %all-gather.38.cloned.1.call-done = bf16[2048,1024]{1,0:T(8,128)(2,1)} async-done(((bf16[512,1024]{1,0:T(8,128)(2,1)}), bf16[2048,1024]{1,0:T(8,128)(2,1)}) %all-gather.38.cloned.1.call-update) | async-done | bytes 4194320 | tf_op jit(solution)/shard_map/all_gather | solution.py:210
  480.8 5.3 fusion.74
  486.1 40.3 %all-gather.30.cloned.1.call-done = bf16[2048,512]{1,0:T(8,128)(2,1)} async-done(((bf16[512,512]{1,0:T(8,128)(2,1)}), bf16[2048,512]{1,0:T(8,128)(2,1)}) %all-gather.30.cloned.1.call-update) | async-done | bytes 2097168 | tf_op jit(solution)/shard_map/all_gather | solution.py:209
  526.4 3.4 fusion.16
  529.8 7.3 %reduce-scatter.2.cloned.1.call-done = bf16[128,2048]{1,0:T(8,128)(2,1)} async-done(((bf16[256,2048]{1,0:T(8,128)(2,1)}), bf16[128,2048]{1,0:T(8,128)(2,1)}) %reduce-scatter.2.cloned.1.call-update) | async-done | bytes 524304 | tf_op jit(solution)/shard_map/reduce_scatter | solution.py:312
  (204 shorter events, 15.7 us)
Async XLA Ops:
  6.5 26.4 %copy-start.3 = (bf16[128,512]{1,0:T(8,128)(2,1)S(1)}, bf16[128,512]{1,0:T(8,128)(2,1)}, u32[]{:S(2)}) copy-start(bf16[128,512]{1,0:T(8,128)(2,1)} %param.21) | copy-start | bytes 393220
  6.5 37.0 %copy-start.4 = (bf16[128,512]{1,0:T(8,128)(2,1)S(1)}, bf16[128,512]{1,0:T(8,128)(2,1)}, u32[]{:S(2)}) copy-start(bf16[128,512]{1,0:T(8,128)(2,1)} %param.24) | copy-start | bytes 393220
  6.5 59.4 %all-gather.24.cloned.1.call-start = ((), (), s32[]{:S(2)}) async-start(), calls=%async_computation.2 | async-start | bytes 2621440 | tf_op jit(solution)/shard_map/all_gather | solution.py:205
  19.9 34.3 %copy-start.6 = (bf16[4,4,2048]{2,1,0:T(4,128)(2,1)S(1)}, bf16[4,4,2048]{2,1,0:T(4,128)(2,1)}, u32[]{:S(2)}) copy-start(bf16[4,4,2048]{2,1,0:T(4,128)(2,1)} %param.25) | copy-start | bytes 196612
  19.9 34.3 %copy-start.28 = (f32[4,4]{1,0:T(4,128)S(1)}, f32[4,4]{1,0:T(4,128)}, u32[]{:S(2)}) copy-start(f32[4,4]{1,0:T(4,128)} %param.26) | copy-start | bytes 196
  19.9 34.4 %copy-start = (bf16[1,256,2048]{2,1,0:T(8,128)(2,1)S(1)}, bf16[1,256,2048]{2,1,0:T(8,128)(2,1)}, u32[]{:S(2)}) copy-start(bf16[1,256,2048]{2,1,0:T(8,128)(2,1)} %param.19) | copy-start | bytes 3145732
  19.9 92.1 %all-gather.22.cloned.1.call-start = ((), (), s32[]{:S(2)}) async-start(), calls=%async_computation.1 | async-start | bytes 2621440 | tf_op jit(solution)/shard_map/all_gather | solution.py:206
  31.5 23.0 %copy-start.34 = (f32[2048]{0:T(1024)S(1)}, f32[2048]{0:T(1024)}, u32[]{:S(2)}) copy-start(f32[2048]{0:T(1024)} %param.20) | copy-start | bytes 24580
  31.5 107.7 %all-gather.32.cloned.1.call-start = ((), (), s32[]{:S(2)}) async-start(), calls=%async_computation.6 | async-start | bytes 1310720 | tf_op jit(solution)/shard_map/all_gather | solution.py:199
  32.3 135.2 %all-gather.36.cloned.1.call-start = ((), (), s32[]{:S(2)}) async-start(), calls=%async_computation.8 | async-start | bytes 1310720 | tf_op jit(solution)/shard_map/all_gather | solution.py:201
  32.8 193.5 %all-gather.26.cloned.1.call-start = ((), (), s32[]{:S(2)}) async-start(), calls=%async_computation.3 | async-start | bytes 2621440 | tf_op jit(solution)/shard_map/all_gather | solution.py:204
  43.4 11.7 %slice-start = ((f32[1,2,4,256]{3,2,1,0:T(4,128)}), f32[1,1,4,256]{3,2,1,0:T(4,128)S(1)}, s32[]{:S(2)}) async-start(f32[1,2,4,256]{3,2,1,0:T(4,128)} %param.27), calls=%async_computation.13 | async-start | bytes 8192 | tf_op jit(solution)/shard_map/slice | solution.py:235
  43.4 13.7 %copy-start.7 = (f32[1,2,4,256]{3,2,1,0:T(4,128)S(1)}, f32[1,2,4,256]{3,2,1,0:T(4,128)}, u32[]{:S(2)}) copy-start(f32[1,2,4,256]{3,2,1,0:T(4,128)} %param.27) | copy-start | bytes 24580
  43.5 217.5 %all-gather.28.cloned.1.call-start = ((), (), s32[]{:S(2)}) async-start(), calls=%async_computation.4 | async-start | bytes 2621440 | tf_op jit(solution)/shard_map/all_gather | solution.py:207
  54.1 235.2 %all-gather.40.cloned.1.call-start = ((), (), s32[]{:S(2)}) async-start(), calls=%async_computation.11 | async-start | bytes 1310720 | tf_op jit(solution)/shard_map/all_gather | solution.py:14
  54.6 206.3 %copy-start.30 = (f32[256]{0:T(256)}, f32[256]{0:T(256)S(1)}, u32[]{:S(2)}) copy-start(f32[256]{0:T(256)S(1)} %add_rsqrt_fusion.1) | copy-start | bytes 3076
  68.3 132.7 %copy-start.2 = (bf16[32,4,8,128]{3,2,1,0:T(8,128)(2,1)}, bf16[32,4,8,128]{3,2,1,0:T(8,128)(2,1)S(1)}, u32[]{:S(2)}) copy-start(bf16[32,4,8,128]{3,2,1,0:T(8,128)(2,1)S(1)} %fusion.36) | copy-start | bytes 786436
  116.2 202.0 %all-gather.42.cloned.1.call-start = ((), (), s32[]{:S(2)}) async-start(), calls=%async_computation.12 | async-start | bytes 1310720 | tf_op jit(solution)/shard_map/all_gather | solution.py:14
  118.9 48.7 %copy-start.5 = (bf16[128,512]{1,0:T(8,128)(2,1)S(1)}, bf16[128,512]{1,0:T(8,128)(2,1)}, u32[]{:S(2)}) copy-start(bf16[128,512]{1,0:T(8,128)(2,1)} %param.32) | copy-start | bytes 393220
  119.5 64.3 %copy-start.37 = (u32[32]{0:T(128)S(1)}, u32[32]{0:T(128)}, u32[]{:S(2)}) copy-start(u32[32]{0:T(128)} %constant.215) | copy-start | bytes 388
  121.4 278.6 %all-gather.34.cloned.1.call-start = ((), (), s32[]{:S(2)}) async-start(), calls=%async_computation.7 | async-start | bytes 5242880 | tf_op jit(solution)/shard_map/all_gather | solution.py:208
  139.2 341.4 %all-gather.38.cloned.1.call-start = ((), (), s32[]{:S(2)}) async-start(), calls=%async_computation.9 | async-start | bytes 5242880 | tf_op jit(solution)/shard_map/all_gather | solution.py:210
  167.5 358.9 %all-gather.30.cloned.1.call-start = ((), (), s32[]{:S(2)}) async-start(), calls=%async_computation.5 | async-start | bytes 2621440 | tf_op jit(solution)/shard_map/all_gather | solution.py:209
  178.2 359.0 %reduce-scatter.2.cloned.1.call-start = ((), (), s32[]{:S(2)}) async-start(), calls=%async_computation.10 | async-start | bytes 1572864 | tf_op jit(solution)/shard_map/reduce_scatter | solution.py:312
  318.3 7.6 %copy-start.8 = (f32[1,2,4,128]{3,2,1,0:T(4,128)S(1)}, f32[1,2,4,128]{3,2,1,0:T(4,128)}, u32[]{:S(2)}) copy-start(f32[1,2,4,128]{3,2,1,0:T(4,128)} %param.29) | copy-start | bytes 12292
  318.3 7.6 %copy-start.29 = (f32[4]{0:T(128)S(1)}, f32[4]{0:T(128)}, u32[]{:S(2)}) copy-start(f32[4]{0:T(128)} %get-tuple-element.608) | copy-start | bytes 52
  318.3 7.6 %copy-start.32 = (f32[4]{0:T(128)S(1)}, f32[4]{0:T(128)}, u32[]{:S(2)}) copy-start(f32[4]{0:T(128)} %subtract_exponential_fusion.10) | copy-start | bytes 52
  326.6 1.1 copy-start.33
  327.4 6.7 %copy-start.1 = (bf16[4,256,256]{1,2,0:T(8,128)(2,1)S(1)}, bf16[4,256,256]{1,2,0:T(8,128)(2,1)}, u32[]{:S(2)}) copy-start(bf16[4,256,256]{1,2,0:T(8,128)(2,1)} %get-tuple-element.632) | copy-start | bytes 1572868
  334.1 65.9 %copy-start.31 = (f32[256]{0:T(256)S(1)}, f32[256]{0:T(256)}, u32[]{:S(2)}) copy-start(f32[256]{0:T(256)} %copy-done.30) | copy-start | bytes 3076
  334.1 65.9 %copy-start.35 = (f32[2048]{0:T(1024)S(1)}, f32[2048]{0:T(1024)}, u32[]{:S(2)}) copy-start(f32[2048]{0:T(1024)} %param.20) | copy-start | bytes 24580
  336.1 70.2 %copy-start.27 = (f32[4,128]{1,0:T(4,128)S(1)}, f32[4,128]{1,0:T(4,128)}, u32[]{:S(2)}) copy-start(f32[4,128]{1,0:T(4,128)} %param.30) | copy-start | bytes 6148
  403.5 77.2 %copy-start.9 = (s32[1024]{0:T(1024)S(1)}, s32[1024]{0:T(1024)}, u32[]{:S(2)}) copy-start(s32[1024]{0:T(1024)} %get-tuple-element.635) | copy-start | bytes 12292
  403.5 77.2 %copy-start.10 = (s32[1024]{0:T(1024)S(1)}, s32[1024]{0:T(1024)}, u32[]{:S(2)}) copy-start(s32[1024]{0:T(1024)} %get-tuple-element.636) | copy-start | bytes 12292
  403.5 77.2 %copy-start.11 = (f32[1024]{0:T(1024)S(1)}, f32[1024]{0:T(1024)}, u32[]{:S(2)}) copy-start(f32[1024]{0:T(1024)} %get-tuple-element.637) | copy-start | bytes 12292
  403.5 77.2 %copy-start.12 = (f32[1024]{0:T(1024)S(1)}, f32[1024]{0:T(1024)}, u32[]{:S(2)}) copy-start(f32[1024]{0:T(1024)} %get-tuple-element.638) | copy-start | bytes 12292
  403.5 77.2 %copy-start.13 = (f32[1024]{0:T(1024)S(1)}, f32[1024]{0:T(1024)}, u32[]{:S(2)}) copy-start(f32[1024]{0:T(1024)} %get-tuple-element.639) | copy-start | bytes 12292
  403.5 77.2 %copy-start.14 = (f32[1024]{0:T(1024)S(1)}, f32[1024]{0:T(1024)}, u32[]{:S(2)}) copy-start(f32[1024]{0:T(1024)} %get-tuple-element.640) | copy-start | bytes 12292
  403.5 77.2 %copy-start.15 = (f32[1024]{0:T(1024)S(1)}, f32[1024]{0:T(1024)}, u32[]{:S(2)}) copy-start(f32[1024]{0:T(1024)} %get-tuple-element.641) | copy-start | bytes 12292
  403.5 77.2 %copy-start.16 = (f32[1024]{0:T(1024)S(1)}, f32[1024]{0:T(1024)}, u32[]{:S(2)}) copy-start(f32[1024]{0:T(1024)} %get-tuple-element.642) | copy-start | bytes 12292
  403.6 77.2 %copy-start.17 = (f32[1024]{0:T(1024)S(1)}, f32[1024]{0:T(1024)}, u32[]{:S(2)}) copy-start(f32[1024]{0:T(1024)} %get-tuple-element.643) | copy-start | bytes 12292
  403.6 77.2 %copy-start.18 = (f32[1024]{0:T(1024)S(1)}, f32[1024]{0:T(1024)}, u32[]{:S(2)}) copy-start(f32[1024]{0:T(1024)} %get-tuple-element.644) | copy-start | bytes 12292
  403.6 77.2 %copy-start.19 = (f32[1024]{0:T(1024)S(1)}, f32[1024]{0:T(1024)}, u32[]{:S(2)}) copy-start(f32[1024]{0:T(1024)} %get-tuple-element.645) | copy-start | bytes 12292
  403.6 77.2 %copy-start.20 = (f32[1024]{0:T(1024)S(1)}, f32[1024]{0:T(1024)}, u32[]{:S(2)}) copy-start(f32[1024]{0:T(1024)} %get-tuple-element.646) | copy-start | bytes 12292
  403.6 77.2 %copy-start.21 = (f32[1024]{0:T(1024)S(1)}, f32[1024]{0:T(1024)}, u32[]{:S(2)}) copy-start(f32[1024]{0:T(1024)} %get-tuple-element.647) | copy-start | bytes 12292
  403.6 77.2 %copy-start.22 = (f32[1024]{0:T(1024)S(1)}, f32[1024]{0:T(1024)}, u32[]{:S(2)}) copy-start(f32[1024]{0:T(1024)} %get-tuple-element.648) | copy-start | bytes 12292
  403.6 77.2 %copy-start.23 = (f32[1024]{0:T(1024)S(1)}, f32[1024]{0:T(1024)}, u32[]{:S(2)}) copy-start(f32[1024]{0:T(1024)} %get-tuple-element.649) | copy-start | bytes 12292
  403.6 77.2 %copy-start.24 = (f32[1024]{0:T(1024)S(1)}, f32[1024]{0:T(1024)}, u32[]{:S(2)}) copy-start(f32[1024]{0:T(1024)} %get-tuple-element.650) | copy-start | bytes 12292
  403.6 77.2 %copy-start.25 = (f32[1024]{0:T(1024)S(1)}, f32[1024]{0:T(1024)}, u32[]{:S(2)}) copy-start(f32[1024]{0:T(1024)} %get-tuple-element.651) | copy-start | bytes 12292
  403.6 77.2 %copy-start.26 = (f32[1024]{0:T(1024)S(1)}, f32[1024]{0:T(1024)}, u32[]{:S(2)}) copy-start(f32[1024]{0:T(1024)} %get-tuple-element.652) | copy-start | bytes 12292
  403.7 77.2 %copy-start.36 = (s32[256]{0:T(256)S(1)}, s32[256]{0:T(256)}, u32[]{:S(2)}) copy-start(s32[256]{0:T(256)} %iota_add_fusion.1) | copy-start | bytes 3076
  403.7 2.8 collective-permute-start
  405.0 5.7 %collective-permute-start.1 = (bf16[8,1024]{1,0:T(8,128)(2,1)S(1)}, bf16[8,1024]{1,0:T(8,128)(2,1)S(1)}, u32[]{:S(2)}, u32[]{:S(2)}) collective-permute-start(bf16[8,1024]{1,0:T(8,128)(2,1)S(1)} %get-tuple-element.621), channel_id=1, source_target_pairs={{8,0},{16,8},{24,16},{9,1},{17,9},{25,17},{10,2},{18,10},{26,18},{... | collective-permute-start | bytes 49160 | tf_op jit(solution)/shard_map/ppermute | solution.py:36
Sparse Core Ops, SparseCore 0:
  20.0 45.9 all-gather.23
  67.5 44.4 all-gather.21
  113.8 25.3 all-gather.31
  140.9 26.4 all-gather.35
  168.9 46.0 all-gather.25
  216.4 44.4 all-gather.27
  262.5 26.7 all-gather.39
  290.9 27.3 all-gather.41
  319.8 80.1 all-gather.33
  401.4 79.2 all-gather.37
  482.2 44.1 all-gather.29
  529.9 7.1 reduce-scatter.1
where the time goes:
time: 545 us; the launch traced here: 544 us
  waiting for transfers between devices  359 us (66%)
  blocking collectives  93.4 us (17%)
  matrix products  34.2 us (6%)
  other arithmetic  26.8 us (5%)
  between operations  15 us (3%)
  local copies, waits for them, and re-layouts  12.1 us (2%)
    all_gather x1, waiting for transfers between devices, per_device(): lax.all_gather(line_pool_out, 'sp', axis=0, tiled=True)  69.9 us
    all_gather x1, waiting for transfers between devices, per_device(): lax.all_gather(line_pool, 'sp', axis=0, tiled=True)  63.9 us
    all_gather x1, waiting for transfers between devices, per_device(): lax.all_gather(line_value, 'sp', axis=0, tiled=True)  43.7 us
    all_gather x2, waiting for transfers between devices, carried_in(): everything = jax.tree.map(lambda part: lax.all_gather(part, axis), x)  42.1 us
    all_gather x1, waiting for transfers between devices, per_device(): lax.all_gather(line_mem_out, 'sp', axis=0, tiled=True)  40.3 us
    all_gather x1, waiting for transfers between devices, per_device(): lax.all_gather(line_outgate, 'sp', axis=0, tiled=True)  31.8 us
    all_gather x1, waiting for transfers between devices, per_device(): lax.all_gather(pool_out_weight, 'fs', axis=0, tiled=True)  28.2 us
    all_gather x2, blocking collectives, carried_in(): everything = jax.tree.map(lambda part: lax.all_gather(part, axis), x)  24.6 us
  transfers between devices with their start and end apart: 14, of which 12 were waited for; matrix products, arithmetic and copies ran while one was open for 13% of the time, Pallas kernels for 0%

commit v1 on v0

--- a/solution.py
+++ b/solution.py
@@ -200,11 +200,41 @@
         lax.all_gather(mem_out_weight, "fs", axis=0, tiled=True),
         lax.all_gather(pool_out_weight, "fs", axis=0, tiled=True),
     )
+
+    def obtain_gates(k_dim, my_data):
+        across = "sp"
+        parts_out = lax.axis_size(across)
+        fresh = lax.axis_index(across)
+        part_now, back, later = (parts_out, fresh, my_data.shape[k_dim])
+        all_rows = []
+        for c in range(part_now):
+            all_rows.append((c, (c + 1) % part_now))
+        pile = []
+        for c in range(part_now):
+            pile.append((c, (c - 1) % part_now))
+        known = jnp.zeros(
+            (*my_data.shape[:k_dim], part_now * later, *my_data.shape[k_dim + 1 :]), my_data.dtype
+        )
+        piece_now = next_value = my_data
+        known = lax.dynamic_update_slice_in_dim(known, my_data, back * later, axis=k_dim)
+        upper = part_now // 2
+        for w in range(1, upper + 1):
+            piece_now = lax.ppermute(piece_now, axis_name=across, perm=all_rows)
+            known = lax.dynamic_update_slice_in_dim(
+                known, piece_now, (back - w) % part_now * later, axis=k_dim
+            )
+            if w < part_now - upper:
+                next_value = lax.ppermute(next_value, axis_name=across, perm=pile)
+                known = lax.dynamic_update_slice_in_dim(
+                    known, next_value, (back + w) % part_now * later, axis=k_dim
+                )
+        return known
+
     pieces = (
         lax.all_gather(line_query, "sp", axis=0, tiled=True),
         lax.all_gather(line_key, "sp", axis=0, tiled=True),
         lax.all_gather(line_value, "sp", axis=0, tiled=True),
-        lax.all_gather(line_outgate, "sp", axis=0, tiled=True),
+        obtain_gates(0, my_data=line_outgate),
         lax.all_gather(line_pool, "sp", axis=0, tiled=True),
         lax.all_gather(line_mem_out, "sp", axis=0, tiled=True),
         lax.all_gather(line_pool_out, "sp", axis=0, tiled=True),

time: 545 us -> 523 us (0.960)
  waiting for transfers between devices: 359 us -> 311 us
  blocking collectives: 93.4 us -> 112 us
    all_gather x2, waiting for transfers between devices: 42.1 us -> 3.41 us  [carried_in(): everything = jax.tree.map(lambda part: lax.all_gather(part, axis), x)]
    all_gather x1 -> x0, waiting for transfers between devices: 31.8 us -> none  [per_device(): lax.all_gather(line_outgate, 'sp', axis=0, tiled=True)]
    unnamed x1, blocking collectives: 12.3 us -> 32.5 us
    all_gather x1, waiting for transfers between devices: 8.72 us -> 20.2 us  [per_device(): lax.all_gather(line_key, 'sp', axis=0, tiled=True)]
    ppermute x0 -> x3, waiting for transfers between devices: none -> 11 us  [the longest x2 11 us: obtain_gates(): piece_now = lax.ppermute(piece_now, axis_name=across, perm=all_rows)]
  transfers between devices with their start and end apart: 14 -> 16, of which waited for: 12 -> 11; matrix products, arithmetic and copies ran while one was open for 13% -> 14% of each run, Pallas kernels for 0% -> 0%
where the time goes in v1:
time: 523 us; the launch traced here: 521 us
  waiting for transfers between devices  311 us (59%)
  blocking collectives  112 us (21%)
  matrix products  33 us (6%)
  other arithmetic  27 us (5%)
  local copies, waits for them, and re-layouts  16.1 us (3%)
  between operations  14.8 us (3%)
  starting transfers between devices  6.84 us (1%)
    all_gather x1, waiting for transfers between devices, per_device(): lax.all_gather(line_pool_out, 'sp', axis=0, tiled=True)  70 us
    all_gather x1, waiting for transfers between devices, per_device(): lax.all_gather(line_pool, 'sp', axis=0, tiled=True)  63.9 us
    all_gather x1, waiting for transfers between devices, per_device(): lax.all_gather(line_value, 'sp', axis=0, tiled=True)  43.7 us
    all_gather x1, waiting for transfers between devices, per_device(): lax.all_gather(line_mem_out, 'sp', axis=0, tiled=True)  40.1 us
    unnamed x1, blocking collectives  32.5 us
    all_gather x1, waiting for transfers between devices, per_device(): lax.all_gather(pool_out_weight, 'fs', axis=0, tiled=True)  28.2 us
    all_gather x2, blocking collectives, carried_in(): everything = jax.tree.map(lambda part: lax.all_gather(part, axis), x)  24.4 us
    all_gather x1, waiting for transfers between devices, per_device(): lax.all_gather(line_key, 'sp', axis=0, tiled=True)  20.2 us
  transfers between devices with their start and end apart: 16, of which 11 were waited for; matrix products, arithmetic and copies ran while one was open for 14% of the time, Pallas kernels for 0%

profile of v1, /device:TPU:0, one launch (start us, length us, event | category | flops | bytes accessed | tf_op | source)
XLA Modules:
  0.0 520.8 jit_solution(9403060173089352101)
XLA Ops:
  6.6 13.3 %all_gather.86 = bf16[512,512]{1,0:T(8,128)(2,1)} all-gather(bf16[128,512]{1,0:T(8,128)(2,1)} %param.22), channel_id=1, replica_groups=mesh['sp'=4,'fs'=4,'tp'=2] {'fs'}, dimensions={0}, use_global_device_ids=true | all-gather | bytes 655360 | tf_op jit(solution)/shard_map/all_gather | solution.py:196
  20.0 11.4 %all_gather.84 = bf16[512,512]{1,0:T(8,128)(2,1)} all-gather(bf16[128,512]{1,0:T(8,128)(2,1)} %param.23), channel_id=1, replica_groups=mesh['sp'=4,'fs'=4,'tp'=2] {'fs'}, dimensions={0}, use_global_device_ids=true | all-gather | bytes 655360 | tf_op jit(solution)/shard_map/all_gather | solution.py:197
  31.5 0.7 all-gather.29.cloned.1.call-update
  32.8 9.8 %all_gather.92 = bf16[512,512]{1,0:T(8,128)(2,1)} all-gather(bf16[128,512]{1,0:T(8,128)(2,1)S(1)} %copy-done.3), channel_id=1, replica_groups=mesh['sp'=4,'fs'=4,'tp'=2] {'fs'}, dimensions={0}, use_global_device_ids=true | all-gather | bytes 655360 | tf_op jit(solution)/shard_map/all_gather | solution.py:195
  43.7 1.2 reduce-window.24
  45.8 20.2 %all-gather.23.cloned.1.call-done = bf16[2048,512]{1,0:T(8,128)(2,1)} async-done(((bf16[512,512]{1,0:T(8,128)(2,1)}), bf16[2048,512]{1,0:T(8,128)(2,1)}) %all-gather.23.cloned.1.call-update) | async-done | bytes 2097168 | tf_op jit(solution)/shard_map/all_gather | solution.py:235
  66.0 2.3 fusion.36
  68.3 43.7 %all-gather.21.cloned.1.call-done = bf16[2048,512]{1,0:T(8,128)(2,1)} async-done(((bf16[512,512]{1,0:T(8,128)(2,1)}), bf16[2048,512]{1,0:T(8,128)(2,1)}) %all-gather.21.cloned.1.call-update) | async-done | bytes 2097168 | tf_op jit(solution)/shard_map/all_gather | solution.py:236
  112.1 2.3 fusion.35
  114.4 1.9 fusion.71
  116.6 1.2 reduce-window.26
  119.6 1.9 fusion.65
  121.6 17.6 %all-gather.29.cloned.1.call-done = bf16[512,1024]{1,0:T(8,128)(2,1)} async-done(((bf16[128,1024]{1,0:T(8,128)(2,1)}), bf16[512,1024]{1,0:T(8,128)(2,1)}) %all-gather.29.cloned.1.call-update) | async-done | bytes 1048592 | tf_op jit(solution)/shard_map/all_gather | solution.py:199
  139.3 28.2 %all-gather.33.cloned.1.call-done = bf16[512,1024]{1,0:T(8,128)(2,1)} async-done(((bf16[128,1024]{1,0:T(8,128)(2,1)}), bf16[512,1024]{1,0:T(8,128)(2,1)}) %all-gather.33.cloned.1.call-update) | async-done | bytes 1048592 | tf_op jit(solution)/shard_map/all_gather | solution.py:201
  167.5 10.1 %all_gather.101 = bf16[512,512]{1,0:T(8,128)(2,1)S(1)} all-gather(bf16[128,512]{1,0:T(8,128)(2,1)S(1)} %copy-done.4), channel_id=1, replica_groups=mesh['sp'=4,'fs'=4,'tp'=2] {'fs'}, dimensions={0}, use_global_device_ids=true | all-gather | bytes 655360 | tf_op jit(solution)/shard_map/all_gather | solution.py:198
  177.6 1.5 collective-permute-start
  179.1 2.3 collective-permute-start.1
  181.4 10.5 %all_gather.102 = bf16[512,512]{1,0:T(8,128)(2,1)} all-gather(bf16[128,512]{1,0:T(8,128)(2,1)S(1)} %copy-done.5), channel_id=1, replica_groups=mesh['sp'=4,'fs'=4,'tp'=2] {'fs'}, dimensions={0}, use_global_device_ids=true | all-gather | bytes 655360 | tf_op jit(solution)/shard_map/all_gather | solution.py:200
  197.9 32.5 %all-reduce.4 = (f32[16]{0:T(128)S(1)}, f32[16]{0:T(128)S(1)}, f32[16]{0:T(128)S(1)}, f32[16]{0:T(128)S(1)}) all-reduce(f32[16]{0:T(128)S(1)} %dynamic-update-slice.2, f32[16]{0:T(128)S(1)} %dynamic-update-slice.3, f32[16]{0:T(128)S(1)} %dynamic-update-slice, f32[16]{0:T(128)S(1)} %dynamic-update-slice.1), channel_id=6, replica_groups=mesh['sp'=4,'fs'=4,'tp'=2] {'sp'}, use_global_device_ids=true, to_apply=%add.2 | all-reduce | flops 64 | bytes 512
  230.4 0.7 reshape.473
  231.1 0.7 reshape.477
  234.5 0.7 fusion.58
  235.3 1.1 constant_dynamic-update-slice_fusion.1
  236.4 11.0 %collective-permute-done.2 = bf16[512,512]{1,0:T(8,128)(2,1)S(1)} collective-permute-done((bf16[512,512]{1,0:T(8,128)(2,1)S(1)}, bf16[512,512]{1,0:T(8,128)(2,1)S(1)}, u32[]{:S(2)}, u32[]{:S(2)}) %collective-permute-start.2) | collective-permute-done | bytes 524320 | tf_op jit(solution)/shard_map/ppermute | solution.py:222
  247.4 0.8 fusion.34
  248.5 1.3 fusion.70
  249.8 12.3 %all-gather.8 = f32[4,4,128]{2,1,0:T(4,128)S(1)} all-gather(f32[1,4,128]{2,1,0:T(4,128)S(1)} %bitcast.306), channel_id=5, replica_groups=mesh['sp'=4,'fs'=4,'tp'=2] {'sp'}, dimensions={0}, use_global_device_ids=true | all-gather | bytes 10240 | tf_op jit(solution)/shard_map/all_gather | solution.py:14
  262.6 12.1 %all-gather.9 = f32[4,4,128]{2,1,0:T(4,128)S(1)} all-gather(f32[1,4,128]{2,1,0:T(4,128)S(1)} %bitcast.302), channel_id=9, replica_groups=mesh['sp'=4,'fs'=4,'tp'=2] {'sp'}, dimensions={0}, use_global_device_ids=true | all-gather | bytes 10240 | tf_op jit(solution)/shard_map/all_gather | solution.py:14
  274.7 2.5 fusion.37
  277.1 0.7 copy.134
  277.9 3.2 rev.25
  281.1 7.5 %while.12 = (s32[]{:T(128)}, f32[4,128,128]{2,1,0:T(8,128)S(1)}, f32[4,128]{1,0:T(4,128)S(1)}, f32[4]{0:T(128)S(1)}, f32[4]{0:T(128)S(1)}, /*index=5*/s32[]{:T(1...) while((s32[]{:T(128)}, f32[4,128,128]{2,1,0:T(8,128)S(1)}, ...), condition=%wide.region_5.6_spmd.clone, body=%wide.region_4.5_spmd.clone.sunk | while | flops 330284 | bytes 792973 | solution.py:25
  281.1 0.7 broadcast_select_fusion.10
  281.8 1.1 fusion.157
  283.0 0.7 broadcast_select_fusion.10
  283.7 1.1 fusion.157
  284.9 0.7 broadcast_select_fusion.10
  285.6 1.1 fusion.157
  286.7 0.7 broadcast_select_fusion.10
  287.4 1.1 fusion.157
  289.8 2.2 fusion.133
  292.0 3.4 all-gather.39.cloned.1.call-done
  295.4 7.5 %while.13 = (s32[]{:T(128)}, f32[4,128,128]{2,1,0:T(8,128)S(1)}, f32[4,128]{1,0:T(4,128)S(1)}, f32[4]{0:T(128)S(1)}, f32[4]{0:T(128)S(1)}, /*index=5*/s32[]{:T(1...) while((s32[]{:T(128)}, f32[4,128,128]{2,1,0:T(8,128)S(1)}, ...), condition=%wide.region_12.13_spmd.clone, body=%wide.region_11.12_spmd.clone.sunk | while | flops 330288 | bytes 793035 | solution.py:25
  295.4 0.7 broadcast_select_fusion.11
  296.2 1.1 fusion.159
  297.3 0.7 broadcast_select_fusion.11
  298.0 1.1 fusion.159
  299.2 0.7 broadcast_select_fusion.11
  299.9 1.1 fusion.159
  301.1 0.7 broadcast_select_fusion.11
  301.8 1.1 fusion.159
  304.9 1.2 fusion.25
  306.1 5.1 rev.26
  311.6 1.7 multiply_reduce_fusion
  313.3 63.9 %all-gather.31.cloned.1.call-done = bf16[2048,1024]{1,0:T(8,128)(2,1)} async-done(((bf16[512,1024]{1,0:T(8,128)(2,1)}), bf16[2048,1024]{1,0:T(8,128)(2,1)}) %all-gather.31.cloned.1.call-update) | async-done | bytes 4194320 | tf_op jit(solution)/shard_map/all_gather | solution.py:238
  377.1 3.5 convolution_convert_fusion
  380.8 1.3 collective-permute-start.3
  382.1 1.3 collective-permute-start.4
  383.6 4.2 collective-permute-done.4
  388.0 70.0 %all-gather.35.cloned.1.call-done = bf16[2048,1024]{1,0:T(8,128)(2,1)} async-done(((bf16[512,1024]{1,0:T(8,128)(2,1)}), bf16[2048,1024]{1,0:T(8,128)(2,1)}) %all-gather.35.cloned.1.call-update) | async-done | bytes 4194320 | tf_op jit(solution)/shard_map/all_gather | solution.py:240
  458.1 5.3 %fusion.74 = f32[256,2048]{1,0:T(8,128)S(1)} fusion(bf16[2048,1024]{1,0:T(8,128)(2,1)} %all-gather.35.cloned.1.call-done, f32[272,1024]{1,0:T(8,128)S(1)} %maximum_convert_fusion, s32[1024]{0:T(1024)S(1)} %copy-done.9, s32[1024]{0:T(1024)S(1)} %copy-done.10, s32[256]{0:T(256)S(1)} %copy-done.38, f32[1024]{0:T(1024)S(1)} %copy-done.11, ...), kind=kOutput, calls=%fused_computation.128 | convolution fusion | flops 1084489728 | bytes 23143424 | tf_op jit(solution)/shard_map/dot_general | solution.py:345
  463.5 40.1 %all-gather.27.cloned.1.call-done = bf16[2048,512]{1,0:T(8,128)(2,1)} async-done(((bf16[512,512]{1,0:T(8,128)(2,1)}), bf16[2048,512]{1,0:T(8,128)(2,1)}) %all-gather.27.cloned.1.call-update) | async-done | bytes 2097168 | tf_op jit(solution)/shard_map/all_gather | solution.py:239
  503.6 3.4 fusion.16
  507.0 7.3 %reduce-scatter.2.cloned.1.call-done = bf16[128,2048]{1,0:T(8,128)(2,1)} async-done(((bf16[256,2048]{1,0:T(8,128)(2,1)}), bf16[128,2048]{1,0:T(8,128)(2,1)}) %reduce-scatter.2.cloned.1.call-update) | async-done | bytes 524304 | tf_op jit(solution)/shard_map/reduce_scatter | solution.py:342
  (216 shorter events, 18.0 us)
Async XLA Ops:
  6.5 26.3 %copy-start.3 = (bf16[128,512]{1,0:T(8,128)(2,1)S(1)}, bf16[128,512]{1,0:T(8,128)(2,1)}, u32[]{:S(2)}) copy-start(bf16[128,512]{1,0:T(8,128)(2,1)} %param.21) | copy-start | bytes 393220
  6.5 36.1 %copy-start.6 = (bf16[4,4,2048]{2,1,0:T(4,128)(2,1)S(1)}, bf16[4,4,2048]{2,1,0:T(4,128)(2,1)}, u32[]{:S(2)}) copy-start(bf16[4,4,2048]{2,1,0:T(4,128)(2,1)} %param.25) | copy-start | bytes 196612
  6.5 36.2 %copy-start.28 = (f32[4,4]{1,0:T(4,128)S(1)}, f32[4,4]{1,0:T(4,128)}, u32[]{:S(2)}) copy-start(f32[4,4]{1,0:T(4,128)} %param.26) | copy-start | bytes 196
  6.5 36.3 %copy-start = (bf16[1,256,2048]{2,1,0:T(8,128)(2,1)S(1)}, bf16[1,256,2048]{2,1,0:T(8,128)(2,1)}, u32[]{:S(2)}) copy-start(bf16[1,256,2048]{2,1,0:T(8,128)(2,1)} %param.19) | copy-start | bytes 3145732
  6.5 59.4 %all-gather.23.cloned.1.call-start = ((), (), s32[]{:S(2)}) async-start(), calls=%async_computation.2 | async-start | bytes 2621440 | tf_op jit(solution)/shard_map/all_gather | solution.py:235
  19.9 23.2 %copy-start.35 = (f32[2048]{0:T(1024)S(1)}, f32[2048]{0:T(1024)}, u32[]{:S(2)}) copy-start(f32[2048]{0:T(1024)} %param.20) | copy-start | bytes 24580
  19.9 92.1 %all-gather.21.cloned.1.call-start = ((), (), s32[]{:S(2)}) async-start(), calls=%async_computation.1 | async-start | bytes 2621440 | tf_op jit(solution)/shard_map/all_gather | solution.py:236
  31.4 107.8 %all-gather.29.cloned.1.call-start = ((), (), s32[]{:S(2)}) async-start(), calls=%async_computation.5 | async-start | bytes 1310720 | tf_op jit(solution)/shard_map/all_gather | solution.py:199
  32.1 135.3 %all-gather.33.cloned.1.call-start = ((), (), s32[]{:S(2)}) async-start(), calls=%async_computation.7 | async-start | bytes 1310720 | tf_op jit(solution)/shard_map/all_gather | solution.py:201
  32.7 10.9 %slice-start = ((f32[1,2,4,256]{3,2,1,0:T(4,128)}), f32[1,1,4,256]{3,2,1,0:T(4,128)S(1)}, s32[]{:S(2)}) async-start(f32[1,2,4,256]{3,2,1,0:T(4,128)} %param.27), calls=%async_computation.12 | async-start | bytes 8192 | tf_op jit(solution)/shard_map/slice | solution.py:265
  32.7 12.9 %copy-start.7 = (f32[1,2,4,256]{3,2,1,0:T(4,128)S(1)}, f32[1,2,4,256]{3,2,1,0:T(4,128)}, u32[]{:S(2)}) copy-start(f32[1,2,4,256]{3,2,1,0:T(4,128)} %param.27) | copy-start | bytes 24580
  32.7 241.9 %all-gather.25.cloned.1.call-start = ((), (), s32[]{:S(2)}) async-start(), calls=%async_computation.3 | async-start | bytes 2621440 | tf_op jit(solution)/shard_map/all_gather | solution.py:234
  42.6 238.5 %all-gather.37.cloned.1.call-start = ((), (), s32[]{:S(2)}) async-start(), calls=%async_computation.10 | async-start | bytes 1310720 | tf_op jit(solution)/shard_map/all_gather | solution.py:14
  43.1 68.9 %copy-start.30 = (f32[256]{0:T(256)}, f32[256]{0:T(256)S(1)}, u32[]{:S(2)}) copy-start(f32[256]{0:T(256)S(1)} %add_rsqrt_fusion.1) | copy-start | bytes 3076
  68.3 50.5 %copy-start.2 = (bf16[32,4,8,128]{3,2,1,0:T(8,128)(2,1)}, bf16[32,4,8,128]{3,2,1,0:T(8,128)(2,1)S(1)}, u32[]{:S(2)}) copy-start(bf16[32,4,8,128]{3,2,1,0:T(8,128)(2,1)S(1)} %fusion.36) | copy-start | bytes 786436
  116.3 179.1 %all-gather.39.cloned.1.call-start = ((), (), s32[]{:S(2)}) async-start(), calls=%async_computation.11 | async-start | bytes 1310720 | tf_op jit(solution)/shard_map/all_gather | solution.py:14
  119.0 48.6 %copy-start.4 = (bf16[128,512]{1,0:T(8,128)(2,1)S(1)}, bf16[128,512]{1,0:T(8,128)(2,1)}, u32[]{:S(2)}) copy-start(bf16[128,512]{1,0:T(8,128)(2,1)} %param.24) | copy-start | bytes 393220
  119.3 62.2 %copy-start.5 = (bf16[128,512]{1,0:T(8,128)(2,1)S(1)}, bf16[128,512]{1,0:T(8,128)(2,1)}, u32[]{:S(2)}) copy-start(bf16[128,512]{1,0:T(8,128)(2,1)} %param.32) | copy-start | bytes 393220
  121.5 74.3 %copy-start.39 = (u32[32]{0:T(128)S(1)}, u32[32]{0:T(128)}, u32[]{:S(2)}) copy-start(u32[32]{0:T(128)} %constant.242) | copy-start | bytes 388
  121.5 255.6 %all-gather.31.cloned.1.call-start = ((), (), s32[]{:S(2)}) async-start(), calls=%async_computation.6 | async-start | bytes 5242880 | tf_op jit(solution)/shard_map/all_gather | solution.py:238
  139.3 318.7 %all-gather.35.cloned.1.call-start = ((), (), s32[]{:S(2)}) async-start(), calls=%async_computation.8 | async-start | bytes 5242880 | tf_op jit(solution)/shard_map/all_gather | solution.py:240
  167.5 336.1 %all-gather.27.cloned.1.call-start = ((), (), s32[]{:S(2)}) async-start(), calls=%async_computation.4 | async-start | bytes 2621440 | tf_op jit(solution)/shard_map/all_gather | solution.py:239
  177.6 56.4 %collective-permute-start = (bf16[512,512]{1,0:T(8,128)(2,1)S(1)}, bf16[512,512]{1,0:T(8,128)(2,1)S(1)}, u32[]{:S(2)}, u32[]{:S(2)}) collective-permute-start(bf16[512,512]{1,0:T(8,128)(2,1)S(1)} %all_gather.101), channel_id=1, source_target_pairs={{0,8},{8,16},{16,24},{24,0},{1,9},{9,17},{17,25},{25,1},{2,10},{10... | collective-permute-start | bytes 1572872 | tf_op jit(solution)/shard_map/ppermute | solution.py:222
  179.1 56.2 %collective-permute-start.1 = (bf16[512,512]{1,0:T(8,128)(2,1)S(1)}, bf16[512,512]{1,0:T(8,128)(2,1)}, u32[]{:S(2)}, u32[]{:S(2)}) collective-permute-start(bf16[512,512]{1,0:T(8,128)(2,1)S(1)} %all_gather.101), channel_id=1, source_target_pairs={{0,24},{8,0},{16,8},{24,16},{1,25},{9,1},{17,9},{25,17},{2,26},{10... | collective-permute-start | bytes 1572872 | tf_op jit(solution)/shard_map/ppermute | solution.py:227
  192.0 322.4 %reduce-scatter.2.cloned.1.call-start = ((), (), s32[]{:S(2)}) async-start(), calls=%async_computation.9 | async-start | bytes 1572864 | tf_op jit(solution)/shard_map/reduce_scatter | solution.py:342
  233.3 14.1 %copy-start.31 = (f32[256]{0:T(256)S(1)}, f32[256]{0:T(256)}, u32[]{:S(2)}) copy-start(f32[256]{0:T(256)} %copy-done.30) | copy-start | bytes 3076
  233.3 14.1 %copy-start.36 = (f32[2048]{0:T(1024)S(1)}, f32[2048]{0:T(1024)}, u32[]{:S(2)}) copy-start(f32[2048]{0:T(1024)} %param.20) | copy-start | bytes 24580
  234.0 13.4 %collective-permute-start.2 = (bf16[512,512]{1,0:T(8,128)(2,1)S(1)}, bf16[512,512]{1,0:T(8,128)(2,1)S(1)}, u32[]{:S(2)}, u32[]{:S(2)}) collective-permute-start(bf16[512,512]{1,0:T(8,128)(2,1)S(1)} %collective-permute-done), channel_id=1, source_target_pairs={{0,8},{8,16},{16,24},{24,0},{1,9},{9,17},{17,25},{25,1},{2,10},{10... | collective-permute-start | bytes 1572872 | tf_op jit(solution)/shard_map/ppermute | solution.py:222
  295.4 7.6 %copy-start.8 = (f32[1,2,4,128]{3,2,1,0:T(4,128)S(1)}, f32[1,2,4,128]{3,2,1,0:T(4,128)}, u32[]{:S(2)}) copy-start(f32[1,2,4,128]{3,2,1,0:T(4,128)} %param.29) | copy-start | bytes 12292
  295.4 7.6 %copy-start.29 = (f32[4]{0:T(128)S(1)}, f32[4]{0:T(128)}, u32[]{:S(2)}) copy-start(f32[4]{0:T(128)} %get-tuple-element.608) | copy-start | bytes 52
  295.4 7.6 %copy-start.33 = (f32[4]{0:T(128)S(1)}, f32[4]{0:T(128)}, u32[]{:S(2)}) copy-start(f32[4]{0:T(128)} %subtract_exponential_fusion.10) | copy-start | bytes 52
  303.8 1.1 copy-start.34
  304.6 6.7 %copy-start.1 = (bf16[4,256,256]{1,2,0:T(8,128)(2,1)S(1)}, bf16[4,256,256]{1,2,0:T(8,128)(2,1)}, u32[]{:S(2)}) copy-start(bf16[4,256,256]{1,2,0:T(8,128)(2,1)} %get-tuple-element.632) | copy-start | bytes 1572868
  311.3 65.8 %copy-start.32 = (f32[256]{0:T(256)S(1)}, f32[256]{0:T(256)}, u32[]{:S(2)}) copy-start(f32[256]{0:T(256)} %copy-done.30) | copy-start | bytes 3076
  311.3 65.8 %copy-start.37 = (f32[2048]{0:T(1024)S(1)}, f32[2048]{0:T(1024)}, u32[]{:S(2)}) copy-start(f32[2048]{0:T(1024)} %param.20) | copy-start | bytes 24580
  313.3 70.2 %copy-start.27 = (f32[4,128]{1,0:T(4,128)S(1)}, f32[4,128]{1,0:T(4,128)}, u32[]{:S(2)}) copy-start(f32[4,128]{1,0:T(4,128)} %param.30) | copy-start | bytes 6148
  380.6 77.3 %copy-start.9 = (s32[1024]{0:T(1024)S(1)}, s32[1024]{0:T(1024)}, u32[]{:S(2)}) copy-start(s32[1024]{0:T(1024)} %get-tuple-element.635) | copy-start | bytes 12292
  380.6 77.3 %copy-start.10 = (s32[1024]{0:T(1024)S(1)}, s32[1024]{0:T(1024)}, u32[]{:S(2)}) copy-start(s32[1024]{0:T(1024)} %get-tuple-element.636) | copy-start | bytes 12292
  380.6 77.3 %copy-start.11 = (f32[1024]{0:T(1024)S(1)}, f32[1024]{0:T(1024)}, u32[]{:S(2)}) copy-start(f32[1024]{0:T(1024)} %get-tuple-element.637) | copy-start | bytes 12292
  380.7 77.3 %copy-start.12 = (f32[1024]{0:T(1024)S(1)}, f32[1024]{0:T(1024)}, u32[]{:S(2)}) copy-start(f32[1024]{0:T(1024)} %get-tuple-element.638) | copy-start | bytes 12292
  380.7 77.3 %copy-start.13 = (f32[1024]{0:T(1024)S(1)}, f32[1024]{0:T(1024)}, u32[]{:S(2)}) copy-start(f32[1024]{0:T(1024)} %get-tuple-element.639) | copy-start | bytes 12292
  380.7 77.3 %copy-start.14 = (f32[1024]{0:T(1024)S(1)}, f32[1024]{0:T(1024)}, u32[]{:S(2)}) copy-start(f32[1024]{0:T(1024)} %get-tuple-element.640) | copy-start | bytes 12292
  380.7 77.3 %copy-start.15 = (f32[1024]{0:T(1024)S(1)}, f32[1024]{0:T(1024)}, u32[]{:S(2)}) copy-start(f32[1024]{0:T(1024)} %get-tuple-element.641) | copy-start | bytes 12292
  380.7 77.3 %copy-start.16 = (f32[1024]{0:T(1024)S(1)}, f32[1024]{0:T(1024)}, u32[]{:S(2)}) copy-start(f32[1024]{0:T(1024)} %get-tuple-element.642) | copy-start | bytes 12292
  380.7 77.3 %copy-start.17 = (f32[1024]{0:T(1024)S(1)}, f32[1024]{0:T(1024)}, u32[]{:S(2)}) copy-start(f32[1024]{0:T(1024)} %get-tuple-element.643) | copy-start | bytes 12292
  380.7 77.3 %copy-start.18 = (f32[1024]{0:T(1024)S(1)}, f32[1024]{0:T(1024)}, u32[]{:S(2)}) copy-start(f32[1024]{0:T(1024)} %get-tuple-element.644) | copy-start | bytes 12292
  380.7 77.3 %copy-start.19 = (f32[1024]{0:T(1024)S(1)}, f32[1024]{0:T(1024)}, u32[]{:S(2)}) copy-start(f32[1024]{0:T(1024)} %get-tuple-element.645) | copy-start | bytes 12292
  380.7 77.3 %copy-start.20 = (f32[1024]{0:T(1024)S(1)}, f32[1024]{0:T(1024)}, u32[]{:S(2)}) copy-start(f32[1024]{0:T(1024)} %get-tuple-element.646) | copy-start | bytes 12292
  380.7 77.3 %copy-start.21 = (f32[1024]{0:T(1024)S(1)}, f32[1024]{0:T(1024)}, u32[]{:S(2)}) copy-start(f32[1024]{0:T(1024)} %get-tuple-element.647) | copy-start | bytes 12292
  380.8 77.3 %copy-start.22 = (f32[1024]{0:T(1024)S(1)}, f32[1024]{0:T(1024)}, u32[]{:S(2)}) copy-start(f32[1024]{0:T(1024)} %get-tuple-element.648) | copy-start | bytes 12292
  380.8 77.3 %copy-start.23 = (f32[1024]{0:T(1024)S(1)}, f32[1024]{0:T(1024)}, u32[]{:S(2)}) copy-start(f32[1024]{0:T(1024)} %get-tuple-element.649) | copy-start | bytes 12292
  380.8 77.3 %copy-start.24 = (f32[1024]{0:T(1024)S(1)}, f32[1024]{0:T(1024)}, u32[]{:S(2)}) copy-start(f32[1024]{0:T(1024)} %get-tuple-element.650) | copy-start | bytes 12292
  380.8 77.3 %copy-start.25 = (f32[1024]{0:T(1024)S(1)}, f32[1024]{0:T(1024)}, u32[]{:S(2)}) copy-start(f32[1024]{0:T(1024)} %get-tuple-element.651) | copy-start | bytes 12292
  380.8 77.3 %copy-start.26 = (f32[1024]{0:T(1024)S(1)}, f32[1024]{0:T(1024)}, u32[]{:S(2)}) copy-start(f32[1024]{0:T(1024)} %get-tuple-element.652) | copy-start | bytes 12292
  380.8 77.3 %copy-start.38 = (s32[256]{0:T(256)S(1)}, s32[256]{0:T(256)}, u32[]{:S(2)}) copy-start(s32[256]{0:T(256)} %iota_add_fusion.1) | copy-start | bytes 3076
  380.8 2.8 collective-permute-start.3
  382.1 5.7 %collective-permute-start.4 = (bf16[8,1024]{1,0:T(8,128)(2,1)S(1)}, bf16[8,1024]{1,0:T(8,128)(2,1)S(1)}, u32[]{:S(2)}, u32[]{:S(2)}) collective-permute-start(bf16[8,1024]{1,0:T(8,128)(2,1)S(1)} %get-tuple-element.621), channel_id=1, source_target_pairs={{8,0},{16,8},{24,16},{9,1},{17,9},{25,17},{10,2},{18,10},{26,18},{... | collective-permute-start | bytes 49160 | tf_op jit(solution)/shard_map/ppermute | solution.py:36
Sparse Core Ops, SparseCore 0:
  20.0 45.9 all-gather.22
  67.6 44.4 all-gather.20
  113.9 25.2 all-gather.28
  140.9 26.4 all-gather.32
  168.9 68.8 all-gather.24
  239.2 27.1 all-gather.36
  268.0 27.3 all-gather.38
  297.0 80.1 all-gather.30
  378.7 79.2 all-gather.34
  459.4 44.1 all-gather.26
  507.1 7.1 reduce-scatter.1
